TPU v7x, 32 devices: a whole 2x2x4 slice. The times are simulated.
32 devices in a mesh: fs: 4 (over z), rep: 2 (over y), tp: 4 (over x, core).
Axes of the slice: x: 2, y: 2, z: 4, core: 2. Of those that a mesh axis runs over, the one named last changes fastest.
Arguments:
- saved_hidden: bfloat16 [7168, 2048], P(('fs', 'rep')), may hold values from -12 to 12
- grad_value: bfloat16 [7168, 1024], P(('fs', 'rep'), 'tp'), may hold values from -12 to 12
- saved_mixed: bfloat16 [7168, 1024], P(('fs', 'rep'), 'tp'), may hold values from -12 to 12
- grad_output: bfloat16 [7168, 2048], P(('fs', 'rep')), may hold values from -12 to 12
- basis_value: bfloat16 [2048, 128], replicated, may hold values from -0.5 to 0.5
- basis_output: bfloat16 [2048, 128], replicated, may hold values from -0.5 to 0.5
- weight_value: float32 [2048, 1024], P('fs', 'tp'), may hold values from -0.125 to 0.125
- weight_output: float32 [1024, 2048], P('tp', 'fs'), may hold values from -0.1875 to 0.1875
- first_value: float32 [128, 1024], P('fs', 'tp'), may hold values from -4 to 4
- second_value: float32 [128, 1024], P('fs', 'tp'), may hold values from 0.05 to 0.5
- first_output: float32 [128, 1024], P('fs', 'tp'), may hold values from -4 to 4
- second_output: float32 [128, 1024], P('fs', 'tp'), may hold values from 0.05 to 0.5
Outputs:
- step_value: float32 [2048, 1024], P('fs', 'tp')
- step_output: float32 [1024, 2048], P('tp', 'fs')
- new_weight_value: float32 [2048, 1024], P('fs', 'tp')
- new_weight_output: float32 [1024, 2048], P('tp', 'fs')
- copy_value: bfloat16 [2048, 1024], P(None, 'tp')
- copy_output: bfloat16 [1024, 2048], P('tp')
- new_first_value: float32 [128, 1024], P('fs', 'tp')
- new_second_value: float32 [128, 1024], P('fs', 'tp')
- new_first_output: float32 [128, 1024], P('fs', 'tp')
- new_second_output: float32 [128, 1024], P('fs', 'tp')
All inputs are finite; a program needn't handle non-finite values.
Results may differ from a plain program's by a relative error of at most 0.0045.
Values may be sent and summed in bfloat16 or wider, within the bound.
A program may use at most 64 MiB of HBM per device.

v0:
```python
import jax
import jax.numpy as jnp
from jax import lax
from jax.sharding import PartitionSpec as P

AW = 1024
RANK = 128


first_decay = 0.8
second_decay = 0.9
learning_rate = 0.02
norm_epsilon = 1e-06
contract_leading = (((0,), (0,)), ((), ()))


def moments(projected, first_old, second_old, clip_factor):
    scaled = clip_factor * projected
    first_new = first_decay * first_old + (1.0 - first_decay) * scaled
    second_new = second_decay * second_old + (1.0 - second_decay) * scaled * scaled
    return (first_new, second_new, first_new / jnp.sqrt(second_new))


def split_product(reduced, other):
    upper = reduced.astype(jnp.bfloat16)
    lower = (reduced - upper.astype(jnp.float32)).astype(jnp.bfloat16)
    rank_count = reduced.shape[1]
    stacked = jnp.concatenate([upper, lower], axis=1)
    both = lax.dot_general(stacked, other, contract_leading, preferred_element_type=jnp.float32)
    return both[:rank_count] + both[rank_count:]


def local(
    saved_hidden,
    grad_value,
    saved_mixed,
    grad_output,
    basis_value,
    basis_output,
    weight_value,
    weight_output,
    first_value,
    second_value,
    first_output,
    second_output,
):
    row_count = weight_value.shape[0]
    moment_count = first_value.shape[0]
    fs_index = lax.axis_index("fs")
    row_first = fs_index * row_count
    moment_first = fs_index * moment_count
    value_basis_rows = lax.dynamic_slice_in_dim(basis_value, row_first, row_count, 0).astype(
        jnp.float32
    )
    output_basis_rows = lax.dynamic_slice_in_dim(basis_output, row_first, row_count, 0).astype(
        jnp.float32
    )
    reduced_hidden = jnp.dot(saved_hidden, basis_value, preferred_element_type=jnp.float32)
    reduced_output = jnp.dot(grad_output, basis_output, preferred_element_type=jnp.float32)
    part_value = split_product(reduced_hidden, grad_value)
    part_output = split_product(reduced_output, saved_mixed)
    projected_value, projected_output = lax.psum((part_value, part_output), ("fs", "rep"))
    local_squares = jnp.sum(projected_value * projected_value) + jnp.sum(
        projected_output * projected_output
    )
    total_squares = lax.psum(local_squares, "tp")
    mean_square = total_squares / (2 * RANK * AW)
    clip_factor = jnp.minimum(1.0, 1.0 / jnp.sqrt(mean_square + norm_epsilon))
    value_slice = lax.dynamic_slice_in_dim(projected_value, moment_first, moment_count, 0)
    output_slice = lax.dynamic_slice_in_dim(projected_output, moment_first, moment_count, 0)
    new_first_value, new_second_value, value_direction_rows = moments(
        value_slice, first_value, second_value, clip_factor
    )
    new_first_output, new_second_output, output_direction_rows = moments(
        output_slice, first_output, second_output, clip_factor
    )
    direction_value, direction_output = (
        lax.all_gather(value_direction_rows, "fs", axis=0, tiled=True),
        lax.all_gather(output_direction_rows, "fs", axis=0, tiled=True),
    )
    step_value = jnp.dot(value_basis_rows, direction_value, precision=lax.Precision.HIGHEST)
    step_output = jnp.dot(output_basis_rows, direction_output, precision=lax.Precision.HIGHEST).T
    new_weight_value = weight_value - learning_rate * step_value
    new_weight_output = weight_output - learning_rate * step_output
    copy_value, copy_output = (
        lax.all_gather(new_weight_value.astype(jnp.bfloat16), "fs", axis=0, tiled=True),
        lax.all_gather(new_weight_output.astype(jnp.bfloat16), "fs", axis=1, tiled=True),
    )
    return (
        step_value,
        step_output,
        new_weight_value,
        new_weight_output,
        copy_value,
        copy_output,
        new_first_value,
        new_second_value,
        new_first_output,
        new_second_output,
    )


def solution(mesh):
    return jax.shard_map(
        local,
        mesh=mesh,
        in_specs=(
            P(("fs", "rep"), None),
            P(("fs", "rep"), "tp"),
            P(("fs", "rep"), "tp"),
            P(("fs", "rep"), None),
            P(),
            P(),
            P("fs", "tp"),
            P("tp", "fs"),
            P("fs", "tp"),
            P("fs", "tp"),
            P("fs", "tp"),
            P("fs", "tp"),
        ),
        out_specs=(
            P("fs", "tp"),
            P("tp", "fs"),
            P("fs", "tp"),
            P("tp", "fs"),
            P(None, "tp"),
            P("tp", None),
            P("fs", "tp"),
            P("fs", "tp"),
            P("fs", "tp"),
            P("fs", "tp"),
        ),
        check_vma=False,
    )
```

profile of v0, /device:TPU:0, one launch (start us, length us, event | category | flops | bytes accessed | tf_op | source)
XLA Modules:
  0.0 184.1 jit_solution(20229193853712389)
XLA Ops:
  7.2 0.0 copy-start
  7.2 0.0 all-reduce.3.cloned.1.call-start
  7.3 1.0 copy-done
  8.2 3.4 %subtract_convert_fusion.1 = (bf16[896,128]{0,1:T(8,128)(2,1)S(1)}, bf16[896,128]{0,1:T(8,128)(2,1)S(1)}) fusion(bf16[896,2048]{1,0:T(8,128)(2,1)} %param.12, bf16[2048,128]{1,0:T(8,128)(2,1)S(1)} %copy-done), kind=kOutput, calls=%fused_computation.11 | convolution fusion | flops 470220800 | bytes 4653056 | tf_op jit(solution)/shard_map/dot_general | solution.py:58
  11.6 0.0 copy-start.10
  11.7 0.3 fusion
  12.0 0.0 copy-start.5
  12.0 0.0 copy-start.6
  12.0 0.7 slice_add_fusion.1
  12.7 1.2 subtract_convert_fusion
  13.9 0.0 copy-start.7
  13.9 0.0 copy-start.8
  14.0 0.3 fusion.4
  14.3 0.7 slice_add_fusion
  14.9 0.0 all-reduce.3.cloned.1.call-update
  15.0 0.0 all-gather.3.cloned.1.call-start
  15.0 74.1 %all-reduce.3.cloned.1.call-done = (f32[128,256]{1,0:T(8,128)}, f32[128,256]{1,0:T(8,128)}) async-done(((f32[128,256]{1,0:T(8,128)}, f32[128,256]{1,0:T(8,128)}), (f32[128,256]{1,0:T(8,128)}, f32[128,256]{1,0:T(8,128)})) %all-reduce.3.cloned.1.call-update) | async-done | bytes 262160 | tf_op jit(solution)/shard_map/psum | solution.py:62
  89.1 1.6 multiply_reduce_fusion
  92.0 6.2 %psum.23 = f32[]{:T(128)} all-reduce(f32[]{:T(128)S(6)} %add.41), channel_id=1, replica_groups=mesh['fs'=4,'rep'=2,'tp'=4] {'tp'}, use_global_device_ids=true, to_apply=%region_4.0 | all-reduce | flops 1 | bytes 8 | tf_op jit(solution)/shard_map/psum | solution.py:66
  98.9 1.4 rsqrt_multiply_fusion.1
  100.3 13.4 %all_gather.12 = f32[128,256]{1,0:T(8,128)S(1)} all-gather(f32[32,256]{1,0:T(8,128)S(1)} %get-tuple-element.19), channel_id=1, replica_groups=mesh['fs'=4,'rep'=2,'tp'=4] {'fs'}, dimensions={0}, use_global_device_ids=true | all-gather | bytes 163840 | tf_op jit(solution)/shard_map/all_gather | solution.py:78
  113.7 1.4 fusion.19
  115.1 0.0 all-gather.3.cloned.1.call-update
  115.1 0.0 all-gather.5.cloned.1.call-start
  115.2 1.4 rsqrt_multiply_fusion
  116.6 14.2 %all_gather.13 = f32[128,256]{1,0:T(8,128)S(1)} all-gather(f32[32,256]{1,0:T(8,128)S(1)} %get-tuple-element.16), channel_id=1, replica_groups=mesh['fs'=4,'rep'=2,'tp'=4] {'fs'}, dimensions={0}, use_global_device_ids=true | all-gather | bytes 163840 | tf_op jit(solution)/shard_map/all_gather | solution.py:79
  130.8 1.5 fusion.18
  132.3 0.0 all-gather.5.cloned.1.call-update
  132.3 11.4 %all-gather.3.cloned.1.call-done = bf16[2048,256]{1,0:T(8,128)(2,1)} async-done(((bf16[512,256]{1,0:T(8,128)(2,1)}), bf16[2048,256]{1,0:T(8,128)(2,1)}) %all-gather.3.cloned.1.call-update) | async-done | bytes 1048592 | tf_op jit(solution)/shard_map/all_gather | solution.py:86
  143.7 29.3 %all-gather.5.cloned.1.call-done = bf16[256,2048]{1,0:T(8,128)(2,1)} async-done(((bf16[256,512]{1,0:T(8,128)(2,1)}), bf16[256,2048]{1,0:T(8,128)(2,1)}) %all-gather.5.cloned.1.call-update) | async-done | bytes 1048592 | tf_op jit(solution)/shard_map/all_gather | solution.py:87
  173.0 2.3 %copy.26 = bf16[2048,256]{1,0:T(8,128)(2,1)} copy(bf16[2048,256]{1,0:T(8,128)(2,1)} %all-gather.3.cloned.1.call-done) | data formatting | bytes 2097152
  175.2 2.3 %copy.27 = bf16[256,2048]{1,0:T(8,128)(2,1)} copy(bf16[256,2048]{1,0:T(8,128)(2,1)} %all-gather.5.cloned.1.call-done) | data formatting | bytes 2097152
  (15 shorter events, 0.0 us)
Async XLA Ops:
  7.2 1.0 copy-start
  7.2 4.5 %copy-start.9 = (bf16[896,256]{1,0:T(8,128)(2,1)S(1)}, bf16[896,256]{1,0:T(8,128)(2,1)}, u32[]{:S(2)}) copy-start(bf16[896,256]{1,0:T(8,128)(2,1)} %param.13) | copy-start | bytes 1376260
  7.2 5.5 %copy-start.2 = (bf16[2048,128]{1,0:T(8,128)(2,1)S(1)}, bf16[2048,128]{1,0:T(8,128)(2,1)}, u32[]{:S(2)}) copy-start(bf16[2048,128]{1,0:T(8,128)(2,1)} %param.17) | copy-start | bytes 1572868
  7.2 81.9 %all-reduce.3.cloned.1.call-start = ((), (), s32[]{:S(2)}) async-start(), calls=%async_computation.2 | async-start | bytes 524288 | tf_op jit(solution)/shard_map/psum | solution.py:62
  8.2 4.4 %copy-start.1 = (bf16[896,2048]{1,0:T(8,128)(2,1)S(1)}, bf16[896,2048]{1,0:T(8,128)(2,1)}, u32[]{:S(2)}) copy-start(bf16[896,2048]{1,0:T(8,128)(2,1)} %param.15) | copy-start | bytes 11010052
  11.6 2.3 %copy-start.10 = (bf16[896,256]{1,0:T(8,128)(2,1)S(1)}, bf16[896,256]{1,0:T(8,128)(2,1)}, u32[]{:S(2)}) copy-start(bf16[896,256]{1,0:T(8,128)(2,1)} %param.14) | copy-start | bytes 1376260
  12.0 86.9 %copy-start.5 = (f32[32,256]{1,0:T(8,128)S(1)}, f32[32,256]{1,0:T(8,128)}, u32[]{:S(2)}) copy-start(f32[32,256]{1,0:T(8,128)} %param.21) | copy-start | bytes 98308
  12.0 86.9 %copy-start.6 = (f32[32,256]{1,0:T(8,128)S(1)}, f32[32,256]{1,0:T(8,128)}, u32[]{:S(2)}) copy-start(f32[32,256]{1,0:T(8,128)} %param.20) | copy-start | bytes 98308
  12.7 101.0 %copy-start.3 = (f32[512,256]{1,0:T(8,128)S(1)}, f32[512,256]{1,0:T(8,128)}, u32[]{:S(2)}) copy-start(f32[512,256]{1,0:T(8,128)} %param.18) | copy-start | bytes 1572868
  13.9 101.3 %copy-start.7 = (f32[32,256]{1,0:T(8,128)S(1)}, f32[32,256]{1,0:T(8,128)}, u32[]{:S(2)}) copy-start(f32[32,256]{1,0:T(8,128)} %param.23) | copy-start | bytes 98308
  13.9 101.3 %copy-start.8 = (f32[32,256]{1,0:T(8,128)S(1)}, f32[32,256]{1,0:T(8,128)}, u32[]{:S(2)}) copy-start(f32[32,256]{1,0:T(8,128)} %param.22) | copy-start | bytes 98308
  13.9 116.9 %copy-start.4 = (f32[256,512]{1,0:T(8,128)S(1)}, f32[256,512]{1,0:T(8,128)}, u32[]{:S(2)}) copy-start(f32[256,512]{1,0:T(8,128)} %param.19) | copy-start | bytes 1572868
  15.0 128.7 %all-gather.3.cloned.1.call-start = ((), (), s32[]{:S(2)}) async-start(), calls=%async_computation | async-start | bytes 1310720 | tf_op jit(solution)/shard_map/all_gather | solution.py:86
  115.1 57.8 %all-gather.5.cloned.1.call-start = ((), (), s32[]{:S(2)}) async-start(), calls=%async_computation.1 | async-start | bytes 1310720 | tf_op jit(solution)/shard_map/all_gather | solution.py:87
Sparse Core Ops, SparseCore 0:
  15.1 73.9 all-reduce.2
  115.3 28.3 all-gather.2
  145.8 27.0 all-gather.4
where the time goes:
time: 184 us
  waiting for transfers between devices  115 us (62%)
  blocking collectives  33.7 us (18%)
  between operations  15.9 us (9%)
  matrix products  8.14 us (4%)
  other arithmetic  5.76 us (3%)
  local copies, waits for them, and re-layouts  5.59 us (3%)
    psum x1, waiting for transfers between devices, local(): lax.psum((part_value, part_output), ('fs', 'rep'))  74.1 us
    all_gather x1, waiting for transfers between devices, local(): lax.all_gather(new_weight_output.astype(jnp.bfloat16), 'fs', axis=1, tile...  29.3 us
    all_gather x1, blocking collectives, local(): lax.all_gather(output_direction_rows, 'fs', axis=0, tiled=True)  14.2 us
    all_gather x1, blocking collectives, local(): lax.all_gather(value_direction_rows, 'fs', axis=0, tiled=True)  13.4 us
    all_gather x1, waiting for transfers between devices, local(): lax.all_gather(new_weight_value.astype(jnp.bfloat16), 'fs', axis=0, tiled...  11.4 us
    psum x1, blocking collectives, local(): total_squares = lax.psum(local_squares, 'tp')  6.17 us
    unnamed x24, local copies, waits for them, and re-layouts  5.59 us
  transfers between devices with their start and end apart: 3, of which 3 were waited for; matrix products, arithmetic and copies ran while one was open for 2% of the time, Pallas kernels for 0%

commit v1 on v0

--- a/solution.py
+++ b/solution.py
@@ -1,6 +1,9 @@
+import functools
 import jax
 import jax.numpy as jnp
 from jax import lax
+from jax.experimental import pallas as pl
+from jax.experimental.pallas import tpu as pltpu
 from jax.sharding import PartitionSpec as P
 
 AW = 1024
@@ -100,9 +103,327 @@
     )
 
 
+MESH = pl.DeviceIdType.MESH
+
+
+def remote(src, dst, send, recv, **where):
+    return pltpu.make_async_remote_copy(
+        src_ref=src, dst_ref=dst, send_sem=send, recv_sem=recv, device_id=where, device_id_type=MESH
+    )
+
+
+def exchange(
+    fs_count, rep_count, tp_count,
+    hidden, grad_value, mixed, grad_output, basis_value, basis_output, weight_value, weight_output,
+    first_value, second_value, first_output, second_output,
+    direction, owned, clip, all_value, all_output,
+    tokens_in, thin_in, basis_in, value_in, output_in, moment_in,
+    part, landed, squares_tp, squares_group,
+    load_sem, near_send, near_recv, side_send, side_recv, part_send, part_recv,
+    tp_send, tp_recv, group_send, group_recv, owned_send, owned_recv, turn_send, turn_recv,
+):
+    group = fs_count * rep_count
+    fs, rep, tp = lax.axis_index("fs"), lax.axis_index("rep"), lax.axis_index("tp")
+    me = fs * rep_count + rep
+    tokens = hidden.shape[0]
+    rows = part.shape[2]
+    width = part.shape[3]
+    half = tokens // 2
+
+    loads = []
+
+    def load(source, target):
+        copy = pltpu.make_async_copy(source, target, load_sem.at[len(loads)])
+        copy.start()
+        loads.append(copy)
+        return copy
+
+    weight_loads = [load(weight_value, value_in), load(weight_output, output_in)]
+    stream_loads = []
+    for a, (big, thin, basis) in enumerate(
+        ((hidden, grad_value, basis_value), (grad_output, mixed, basis_output))
+    ):
+        first = load(basis, basis_in.at[a])
+        second = load(thin, thin_in.at[a])
+        blocks = [
+            load(big.at[pl.ds(c * half, half)], tokens_in.at[a, pl.ds(c * half, half)])
+            for c in range(2)
+        ]
+        stream_loads.append((first, second, blocks))
+    moment_loads = [
+        load(source.at[pl.ds(pl.multiple_of(rep * rows, rows), rows)], moment_in.at[i])
+        for i, source in enumerate((first_value, first_output, second_value, second_output))
+    ]
+
+    def member(k):
+        other = lax.rem(me + k, group)
+        return {"fs": other // rep_count, "rep": lax.rem(other, rep_count)}
+
+    barrier = pltpu.get_barrier_semaphore()
+    for k in range(1, group):
+        pl.semaphore_signal(barrier, inc=1, device_id=member(k), device_id_type=MESH)
+    for k in range(1, tp_count):
+        pl.semaphore_signal(
+            barrier, inc=1, device_id={"tp": lax.rem(tp + k, tp_count)}, device_id_type=MESH
+        )
+    for copy in weight_loads:
+        copy.wait()
+    all_value[fs] = value_in[...].astype(jnp.bfloat16)
+    all_output[fs] = output_in[...].astype(jnp.bfloat16)
+    pl.semaphore_wait(barrier, group - 1 + tp_count - 1)
+
+    share_value = value_in.shape[0] // rep_count
+    share_output = output_in.shape[0] // rep_count
+    shares = (
+        (all_value, pl.ds(pl.multiple_of(rep * share_value, share_value), share_value)),
+        (all_output, pl.ds(pl.multiple_of(rep * share_output, share_output), share_output)),
+    )
+    sent = []
+
+    def send(copy):
+        copy.start()
+        sent.append(copy)
+        return copy
+
+    far = {}
+
+    def send_weights(k):
+        far[k] = [
+            send(remote(
+                buffer.at[fs, rows_here], buffer.at[fs, rows_here],
+                near_send.at[a, k - 1], near_recv.at[a, k - 1], fs=lax.rem(fs + k, fs_count),
+            ))
+            for a, (buffer, rows_here) in enumerate(shares)
+        ]
+
+    side = []
+
+    def pass_weights(k):
+        origin = lax.rem(fs + fs_count - k, fs_count)
+        for a, (buffer, rows_here) in enumerate(shares):
+            far[k][a].wait_recv()
+            for j in range(1, rep_count):
+                side.append(send(remote(
+                    buffer.at[origin, rows_here], buffer.at[origin, rows_here],
+                    side_send.at[a, k - 1, j - 1], side_recv.at[a, k - 1, j - 1],
+                    rep=lax.rem(rep + j, rep_count),
+                )))
+
+    near = sorted({1, fs_count - 1})
+    for k in near:
+        send_weights(k)
+
+    parts = []
+    for a in range(2):
+        first, second, blocks = stream_loads[a]
+        first.wait()
+        second.wait()
+        total = None
+        for c in range(2):
+            blocks[c].wait()
+            reduced = jnp.dot(
+                tokens_in[a, pl.ds(c * half, half)], basis_in[a], preferred_element_type=jnp.float32
+            )
+            product = split_product(reduced, thin_in[a, pl.ds(c * half, half)])
+            total = product if total is None else total + product
+        part[a] = total.reshape(group, rows, width)
+        for k in range(1, group):
+            other = lax.rem(me + k, group)
+            parts.append(send(remote(
+                part.at[a, other], landed.at[a, k - 1],
+                part_send.at[a, k - 1], part_recv.at[a, k - 1], **member(k),
+            )))
+
+    for k in range(2, fs_count - 1):
+        send_weights(k)
+    for k in near:
+        pass_weights(k)
+
+    for copy in parts:
+        copy.wait_recv()
+    squares = jnp.zeros((rows, width), jnp.float32)
+    for a in range(2):
+        summed = part[a, me]
+        for k in range(group - 1):
+            summed = summed + landed[a, k]
+        owned[rep, a] = summed
+        squares = squares + summed * summed
+    squares_tp[0] = jnp.full(squares_tp.shape[1:], jnp.sum(squares), jnp.float32)
+    tp_copies = [
+        send(remote(
+            squares_tp.at[0], squares_tp.at[k], tp_send.at[k - 1], tp_recv.at[k - 1],
+            tp=lax.rem(tp + k, tp_count),
+        ))
+        for k in range(1, tp_count)
+    ]
+    owned_copies = [
+        send(remote(
+            owned.at[rep], owned.at[rep], owned_send.at[j - 1], owned_recv.at[j - 1],
+            rep=lax.rem(rep + j, rep_count),
+        ))
+        for j in range(1, rep_count)
+    ]
+    for copy in tp_copies:
+        copy.wait_recv()
+    squares_group[me] = jnp.sum(squares_tp[...], axis=0)
+    group_copies = [
+        send(remote(
+            squares_group.at[me], squares_group.at[me], group_send.at[k - 1], group_recv.at[k - 1],
+            **member(k),
+        ))
+        for k in range(1, group)
+    ]
+    for copy in moment_loads:
+        copy.wait()
+    for copy in group_copies:
+        copy.wait_recv()
+    mean_square = jnp.sum(squares_group[...], axis=0) / (2 * RANK * AW)
+    factor = jnp.minimum(1.0, 1.0 / jnp.sqrt(mean_square + norm_epsilon))
+    clip[...] = factor
+    scale = factor[:1, :1]
+    for a in range(2):
+        _, _, turned = moments(owned[rep, a], moment_in[a], moment_in[2 + a], scale)
+        direction[me, a] = turned.astype(jnp.bfloat16)
+    turn_copies = [
+        send(remote(
+            direction.at[me], direction.at[me], turn_send.at[k - 1], turn_recv.at[k - 1], **member(k)
+        ))
+        for k in range(1, group)
+    ]
+    for k in range(2, fs_count - 1):
+        pass_weights(k)
+    for copy in owned_copies + turn_copies + side:
+        copy.wait_recv()
+    for copy in sent:
+        copy.wait_send()
+
+
+def finish(
+    direction, owned, clip, all_value, all_output, basis_value, basis_output,
+    weight_value, weight_output, first_value, second_value, first_output, second_output,
+    step_value, step_output, new_weight_value, new_weight_output, copy_value, copy_output,
+    new_first_value, new_second_value, new_first_output, new_second_output,
+):
+    fs = lax.axis_index("fs")
+    count = weight_value.shape[0]
+    width = weight_value.shape[1]
+    scale = clip[:1, :1]
+    outputs = ((new_first_value, new_second_value), (new_first_output, new_second_output))
+    for a, (first, second) in enumerate(
+        ((first_value, second_value), (first_output, second_output))
+    ):
+        projected = owned[:, a].reshape(first.shape)
+        new_first, new_second, _ = moments(projected, first[...], second[...], scale)
+        outputs[a][0][...] = new_first
+        outputs[a][1][...] = new_second
+    turn_value = direction[:, 0].reshape(RANK, width)
+    turn_output = direction[:, 1].reshape(RANK, width).astype(jnp.float32).T.astype(jnp.bfloat16)
+    across = (((1,), (1,)), ((), ()))
+
+    def value_step(rows_here):
+        return jnp.dot(basis_value[rows_here], turn_value, preferred_element_type=jnp.float32)
+
+    def output_step(rows_here):
+        return lax.dot_general(
+            turn_output, basis_output[rows_here], across, preferred_element_type=jnp.float32
+        )
+
+    mine = pl.ds(pl.multiple_of(fs * count, count), count)
+    step = value_step(mine)
+    step_value[...] = step
+    new_weight_value[...] = weight_value[...] - learning_rate * step
+    step = output_step(mine)
+    step_output[...] = step
+    new_weight_output[...] = weight_output[...] - learning_rate * step
+    for f in range(all_value.shape[0]):
+        here = pl.ds(f * count, count)
+        copy_value[here] = (
+            all_value[f].astype(jnp.float32) - learning_rate * value_step(here)
+        ).astype(jnp.bfloat16)
+        copy_output[:, here] = (
+            all_output[f].astype(jnp.float32) - learning_rate * output_step(here)
+        ).astype(jnp.bfloat16)
+
+
+def kernels(
+    fs_count, rep_count, tp_count,
+    saved_hidden, grad_value, saved_mixed, grad_output, basis_value, basis_output,
+    weight_value, weight_output, first_value, second_value, first_output, second_output,
+):
+    group = fs_count * rep_count
+    tokens, model = saved_hidden.shape
+    count, width = weight_value.shape
+    rank = basis_value.shape[1]
+    rows = rank // group
+    f32, bf16 = jnp.float32, jnp.bfloat16
+    shape = jax.ShapeDtypeStruct
+    dma = pltpu.SemaphoreType.DMA
+    anywhere = pl.BlockSpec(memory_space=pl.ANY)
+    in_vmem = pl.BlockSpec(memory_space=pltpu.VMEM)
+    direction, owned, clip, all_value, all_output = pl.pallas_call(
+        functools.partial(exchange, fs_count, rep_count, tp_count),
+        out_shape=(
+            shape((group, 2, rows, width), bf16),
+            shape((rep_count, 2, rows, width), f32),
+            shape((8, 128), f32),
+            shape((fs_count, count, width), bf16),
+            shape((fs_count, width, count), bf16),
+        ),
+        in_specs=[anywhere] * 12,
+        out_specs=(in_vmem,) * 5,
+        scratch_shapes=[
+            pltpu.VMEM((2, tokens, model), bf16),
+            pltpu.VMEM((2, tokens, width), bf16),
+            pltpu.VMEM((2, model, rank), bf16),
+            pltpu.VMEM((count, width), f32),
+            pltpu.VMEM((width, count), f32),
+            pltpu.VMEM((4, rows, width), f32),
+            pltpu.VMEM((2, group, rows, width), f32),
+            pltpu.VMEM((2, group - 1, rows, width), f32),
+            pltpu.VMEM((tp_count, 8, 128), f32),
+            pltpu.VMEM((group, 8, 128), f32),
+            dma((14,)),
+            dma((2, fs_count - 1)), dma((2, fs_count - 1)),
+            dma((2, fs_count - 1, rep_count - 1)), dma((2, fs_count - 1, rep_count - 1)),
+            dma((2, group - 1)), dma((2, group - 1)),
+            dma((tp_count - 1,)), dma((tp_count - 1,)),
+            dma((group - 1,)), dma((group - 1,)),
+            dma((rep_count - 1,)), dma((rep_count - 1,)),
+            dma((group - 1,)), dma((group - 1,)),
+        ],
+        compiler_params=pltpu.CompilerParams(
+            collective_id=0, has_side_effects=True, vmem_limit_bytes=32 * 1024 * 1024
+        ),
+        name="exchange",
+    )(
+        saved_hidden, grad_value, saved_mixed, grad_output, basis_value, basis_output,
+        weight_value, weight_output, first_value, second_value, first_output, second_output,
+    )
+    moment = shape(first_value.shape, f32)
+    return pl.pallas_call(
+        finish,
+        out_shape=(
+            shape((count, width), f32), shape((width, count), f32),
+            shape((count, width), f32), shape((width, count), f32),
+            shape((model, width), bf16), shape((width, model), bf16),
+            moment, moment, moment, moment,
+        ),
+        in_specs=[in_vmem] * 13,
+        out_specs=(in_vmem,) * 10,
+        compiler_params=pltpu.CompilerParams(vmem_limit_bytes=32 * 1024 * 1024),
+        name="finish",
+    )(
+        direction, owned, clip, all_value, all_output, basis_value, basis_output,
+        weight_value, weight_output, first_value, second_value, first_output, second_output,
+    )
+
+
 def solution(mesh):
+    fs_count, rep_count, tp_count = mesh.shape["fs"], mesh.shape["rep"], mesh.shape["tp"]
+    whole_tiles = RANK % (16 * fs_count * rep_count) == 0
+    body = functools.partial(kernels, fs_count, rep_count, tp_count) if whole_tiles else local
     return jax.shard_map(
-        local,
+        body,
         mesh=mesh,
         in_specs=(
             P(("fs", "rep"), None),

time: 184 us -> 66.5 us (0.36)
  waiting for transfers between devices: 115 us -> 0 us
  Pallas kernels: 0 us -> 51.8 us
  blocking collectives: 33.7 us -> 0 us
  between operations: 15.9 us -> 0.68 us
  matrix products: 8.14 us -> 0 us
  local copies, waits for them, and re-layouts: 5.59 us -> 13.3 us
  other arithmetic: 5.76 us -> 0 us
    psum x1 -> x0, waiting for transfers between devices: 74.1 us -> none  [local(): lax.psum((part_value, part_output), ('fs', 'rep'))]
    pallas_call x0 -> x2, Pallas kernels: none -> 51.8 us  [the longest x1 48.9 us: kernels(): pl.pallas_call(functools.partial(exchange, fs_count, rep_count, tp_count)...]
    all_gather x2 -> x0, waiting for transfers between devices: 40.7 us -> none  [the longest x1 29.3 us: local(): lax.all_gather(new_weight_output.astype(jnp.bfloat16), 'fs', axis=1, tile...]
    all_gather x2 -> x0, blocking collectives: 27.6 us -> none  [the longest x1 14.2 us: local(): lax.all_gather(output_direction_rows, 'fs', axis=0, tiled=True)]
    dot_general x6 -> x0, matrix products: 8.14 us -> none  [the longest x1 3.4 us: local(): jnp.dot(saved_hidden, basis_value, preferred_element_type=jnp.float32)]
    unnamed x24, local copies, waits for them, and re-layouts: 5.59 us -> 13.3 us
    psum x1 -> x0, blocking collectives: 6.17 us -> none  [local(): total_squares = lax.psum(local_squares, 'tp')]
    div x2 -> x0, other arithmetic: 2.81 us -> none  [moments(): return (first_new, second_new, first_new / jnp.sqrt(second_new))]
  transfers between devices with their start and end apart: 3 -> 0, of which waited for: 3 -> 0; matrix products, arithmetic and copies ran while one was open for 2% -> 0% of each run, Pallas kernels for 0% -> 0%
where the time goes in v1:
time: 66.5 us; the launch traced here: 65.8 us
  Pallas kernels  51.8 us (78%)
  local copies, waits for them, and re-layouts  13.3 us (20%)
  between operations  0.68 us (1%)
    pallas_call x1, Pallas kernels, kernels(): pl.pallas_call(functools.partial(exchange, fs_count, rep_count, tp_count)...  48.9 us
    unnamed x24, local copies, waits for them, and re-layouts  13.3 us
    pallas_call x1, Pallas kernels, kernels(): pl.pallas_call(finish, out_shape=(shape((count, width), f32), shape((widt...  2.87 us

profile of v1, /device:TPU:0, one launch (start us, length us, event | category | flops | bytes accessed | tf_op | source)
XLA Modules:
  0.0 65.8 jit_solution(2138570555515946853)
XLA Ops:
  0.6 0.0 copy-start
  0.7 2.0 %copy-done = bf16[896,2048]{1,0:T(8,128)(2,1)S(1)} copy-done((bf16[896,2048]{1,0:T(8,128)(2,1)S(1)}, bf16[896,2048]{1,0:T(8,128)(2,1)}, u32[]{:S(2)}) %copy-start) | copy-done | bytes 3670040
  2.7 0.0 copy-start.1
  2.7 2.0 %copy-done.1 = bf16[896,2048]{1,0:T(8,128)(2,1)S(1)} copy-done((bf16[896,2048]{1,0:T(8,128)(2,1)S(1)}, bf16[896,2048]{1,0:T(8,128)(2,1)}, u32[]{:S(2)}) %copy-start.1) | copy-done | bytes 3670040
  4.7 0.0 copy-start.2
  4.7 1.0 %copy-done.2 = bf16[2048,128]{1,0:T(8,128)(2,1)S(1)} copy-done((bf16[2048,128]{1,0:T(8,128)(2,1)S(1)}, bf16[2048,128]{1,0:T(8,128)(2,1)}, u32[]{:S(2)}) %copy-start.2) | copy-done | bytes 524312
  5.8 0.0 copy-start.3
  5.8 1.0 %copy-done.3 = bf16[2048,128]{1,0:T(8,128)(2,1)S(1)} copy-done((bf16[2048,128]{1,0:T(8,128)(2,1)S(1)}, bf16[2048,128]{1,0:T(8,128)(2,1)}, u32[]{:S(2)}) %copy-start.3) | copy-done | bytes 524312
  6.8 0.0 copy-start.4
  6.8 1.0 %copy-done.4 = f32[512,256]{1,0:T(8,128)S(1)} copy-done((f32[512,256]{1,0:T(8,128)S(1)}, f32[512,256]{1,0:T(8,128)}, u32[]{:S(2)}) %copy-start.4) | copy-done | bytes 524312
  7.9 0.0 copy-start.5
  7.9 1.0 %copy-done.5 = f32[256,512]{1,0:T(8,128)S(1)} copy-done((f32[256,512]{1,0:T(8,128)S(1)}, f32[256,512]{1,0:T(8,128)}, u32[]{:S(2)}) %copy-start.5) | copy-done | bytes 524312
  8.9 0.0 copy-start.6
  8.9 1.0 %copy-done.6 = bf16[896,256]{1,0:T(8,128)(2,1)S(1)} copy-done((bf16[896,256]{1,0:T(8,128)(2,1)S(1)}, bf16[896,256]{1,0:T(8,128)(2,1)}, u32[]{:S(2)}) %copy-start.6) | copy-done | bytes 458776
  9.9 0.0 copy-start.7
  9.9 1.0 %copy-done.7 = bf16[896,256]{1,0:T(8,128)(2,1)S(1)} copy-done((bf16[896,256]{1,0:T(8,128)(2,1)S(1)}, bf16[896,256]{1,0:T(8,128)(2,1)}, u32[]{:S(2)}) %copy-start.7) | copy-done | bytes 458776
  10.9 0.0 copy-start.8
  10.9 0.8 %copy-done.8 = f32[32,256]{1,0:T(8,128)S(1)} copy-done((f32[32,256]{1,0:T(8,128)S(1)}, f32[32,256]{1,0:T(8,128)}, u32[]{:S(2)}) %copy-start.8) | copy-done | bytes 32792
  11.7 0.0 copy-start.9
  11.7 0.8 %copy-done.9 = f32[32,256]{1,0:T(8,128)S(1)} copy-done((f32[32,256]{1,0:T(8,128)S(1)}, f32[32,256]{1,0:T(8,128)}, u32[]{:S(2)}) %copy-start.9) | copy-done | bytes 32792
  12.4 0.0 copy-start.10
  12.5 0.8 %copy-done.10 = f32[32,256]{1,0:T(8,128)S(1)} copy-done((f32[32,256]{1,0:T(8,128)S(1)}, f32[32,256]{1,0:T(8,128)}, u32[]{:S(2)}) %copy-start.10) | copy-done | bytes 32792
  13.2 0.0 copy-start.11
  13.2 0.8 %copy-done.11 = f32[32,256]{1,0:T(8,128)S(1)} copy-done((f32[32,256]{1,0:T(8,128)S(1)}, f32[32,256]{1,0:T(8,128)}, u32[]{:S(2)}) %copy-start.11) | copy-done | bytes 32792
  14.0 48.9 %exchange.1 = (bf16[8,2,16,256]{3,2,1,0:T(8,128)(2,1)S(1)}, f32[2,2,16,256]{3,2,1,0:T(8,128)S(1)}, f32[8,128]{1,0:T(8,128)S(1)}, bf16[4,512,256]{2,1,0:T(8,128)(2,1)S(1)}, bf16[4,256,512]{2,1,0:T(8,128)(2,1)S(1)}) custom-call(bf16[896,2048]{1,0:T(8,128)(2,1)S(1)} %copy-done, bf16[896,256]{1,0:T(8,128)(2,1)S(1)} %copy-done.6, bf16[896,256]{1,0:T(8,128)(2,1)S(1)} %copy-done.7, ...), custom_call_target="tpu_custom_call" | custom-call | tf_op jit(solution)/shard_map/exchange/pallas_call | solution.py:363
  62.9 2.9 %finish.1 = (f32[512,256]{1,0:T(8,128)}, f32[256,512]{1,0:T(8,128)}, f32[512,256]{1,0:T(8,128)}, f32[256,512]{1,0:T(8,128)}, bf16[2048,256]{1,0:T(8,128)(2,1)}, ...) custom-call(bf16[8,2,16,256]{3,2,1,0:T(8,128)(2,1)S(1)} %get-tuple-e, ...), custom_call_target="tpu_custom_call" | custom-call | tf_op jit(solution)/shard_map/finish/pallas_call | solution.py:403
Async XLA Ops:
  0.6 2.0 %copy-start = (bf16[896,2048]{1,0:T(8,128)(2,1)S(1)}, bf16[896,2048]{1,0:T(8,128)(2,1)}, u32[]{:S(2)}) copy-start(bf16[896,2048]{1,0:T(8,128)(2,1)} %hidden.1) | copy-start | bytes 11010052
  2.7 2.0 %copy-start.1 = (bf16[896,2048]{1,0:T(8,128)(2,1)S(1)}, bf16[896,2048]{1,0:T(8,128)(2,1)}, u32[]{:S(2)}) copy-start(bf16[896,2048]{1,0:T(8,128)(2,1)} %grad_output.1) | copy-start | bytes 11010052
  4.7 1.0 %copy-start.2 = (bf16[2048,128]{1,0:T(8,128)(2,1)S(1)}, bf16[2048,128]{1,0:T(8,128)(2,1)}, u32[]{:S(2)}) copy-start(bf16[2048,128]{1,0:T(8,128)(2,1)} %basis_value.3) | copy-start | bytes 1572868
  5.8 1.0 %copy-start.3 = (bf16[2048,128]{1,0:T(8,128)(2,1)S(1)}, bf16[2048,128]{1,0:T(8,128)(2,1)}, u32[]{:S(2)}) copy-start(bf16[2048,128]{1,0:T(8,128)(2,1)} %basis_output.3) | copy-start | bytes 1572868
  6.8 1.0 %copy-start.4 = (f32[512,256]{1,0:T(8,128)S(1)}, f32[512,256]{1,0:T(8,128)}, u32[]{:S(2)}) copy-start(f32[512,256]{1,0:T(8,128)} %weight_value.3) | copy-start | bytes 1572868
  7.9 1.0 %copy-start.5 = (f32[256,512]{1,0:T(8,128)S(1)}, f32[256,512]{1,0:T(8,128)}, u32[]{:S(2)}) copy-start(f32[256,512]{1,0:T(8,128)} %weight_output.3) | copy-start | bytes 1572868
  8.9 1.0 %copy-start.6 = (bf16[896,256]{1,0:T(8,128)(2,1)S(1)}, bf16[896,256]{1,0:T(8,128)(2,1)}, u32[]{:S(2)}) copy-start(bf16[896,256]{1,0:T(8,128)(2,1)} %grad_value.1) | copy-start | bytes 1376260
  9.9 1.0 %copy-start.7 = (bf16[896,256]{1,0:T(8,128)(2,1)S(1)}, bf16[896,256]{1,0:T(8,128)(2,1)}, u32[]{:S(2)}) copy-start(bf16[896,256]{1,0:T(8,128)(2,1)} %mixed.1) | copy-start | bytes 1376260
  10.9 0.8 %copy-start.8 = (f32[32,256]{1,0:T(8,128)S(1)}, f32[32,256]{1,0:T(8,128)}, u32[]{:S(2)}) copy-start(f32[32,256]{1,0:T(8,128)} %first_value.3) | copy-start | bytes 98308
  11.7 0.8 %copy-start.9 = (f32[32,256]{1,0:T(8,128)S(1)}, f32[32,256]{1,0:T(8,128)}, u32[]{:S(2)}) copy-start(f32[32,256]{1,0:T(8,128)} %second_value.3) | copy-start | bytes 98308
  12.4 0.8 %copy-start.10 = (f32[32,256]{1,0:T(8,128)S(1)}, f32[32,256]{1,0:T(8,128)}, u32[]{:S(2)}) copy-start(f32[32,256]{1,0:T(8,128)} %first_output.3) | copy-start | bytes 98308
  13.2 0.8 %copy-start.11 = (f32[32,256]{1,0:T(8,128)S(1)}, f32[32,256]{1,0:T(8,128)}, u32[]{:S(2)}) copy-start(f32[32,256]{1,0:T(8,128)} %second_output.3) | copy-start | bytes 98308

commit v2 on v1

--- a/solution.py
+++ b/solution.py
@@ -185,33 +185,79 @@
         sent.append(copy)
         return copy
 
-    far = {}
-
-    def send_weights(k):
-        far[k] = [
-            send(remote(
-                buffer.at[fs, rows_here], buffer.at[fs, rows_here],
-                near_send.at[a, k - 1], near_recv.at[a, k - 1], fs=lax.rem(fs + k, fs_count),
-            ))
-            for a, (buffer, rows_here) in enumerate(shares)
-        ]
-
-    side = []
-
-    def pass_weights(k):
-        origin = lax.rem(fs + fs_count - k, fs_count)
-        for a, (buffer, rows_here) in enumerate(shares):
-            far[k][a].wait_recv()
-            for j in range(1, rep_count):
-                side.append(send(remote(
-                    buffer.at[origin, rows_here], buffer.at[origin, rows_here],
-                    side_send.at[a, k - 1, j - 1], side_recv.at[a, k - 1, j - 1],
-                    rep=lax.rem(rep + j, rep_count),
-                )))
-
-    near = sorted({1, fs_count - 1})
-    for k in near:
-        send_weights(k)
+    def hop(a, way, d):
+        buffer, rows_here = shares[a]
+        step = 1 if way == 0 else -1
+        block = buffer.at[fs - step * d, rows_here]
+        return remote(
+            block, block, near_send.at[a, way, d], near_recv.at[a, way, d], fs=fs + step
+        )
+
+    def arrival(a, way, d):
+        buffer, rows_here = shares[a]
+        step = 1 if way == 0 else -1
+        block = buffer.at[fs - step * d, rows_here]
+        return remote(
+            block, block, near_send.at[a, way, d - 1], near_recv.at[a, way, d - 1], fs=fs - step
+        )
+
+    def across(a, way, d, j):
+        buffer, rows_here = shares[a]
+        step = 1 if way == 0 else -1
+        block = buffer.at[fs - step * d, rows_here]
+        return remote(
+            block, block, side_send.at[a, way, d - 1, j - 1], side_recv.at[a, way, d - 1, j - 1],
+            rep=lax.rem(rep + j, rep_count),
+        )
+
+    def reaches(way, d):
+        return fs >= d if way == 0 else fs + d < fs_count
+
+    def leaves(way, d):
+        onward = fs < fs_count - 1 if way == 0 else fs > 0
+        return jnp.logical_and(onward, reaches(way, d))
+
+    def send_weights(d):
+        for way in range(2):
+            @pl.when(leaves(way, d))
+            def _():
+                for a in range(2):
+                    hop(a, way, d).start()
+
+    def pass_weights(d):
+        for a in range(2):
+            for way in range(2):
+                @pl.when(reaches(way, d))
+                def _():
+                    arrival(a, way, d).wait_recv()
+
+                if d < fs_count - 1:
+                    @pl.when(leaves(way, d))
+                    def _():
+                        hop(a, way, d).start()
+
+                @pl.when(reaches(way, d))
+                def _():
+                    for j in range(1, rep_count):
+                        across(a, way, d, j).start()
+
+    def settle_weights():
+        for d in range(fs_count):
+            for way in range(2):
+                if d < fs_count - 1:
+                    @pl.when(leaves(way, d))
+                    def _():
+                        for a in range(2):
+                            hop(a, way, d).wait_send()
+
+                if d > 0:
+                    @pl.when(reaches(way, d))
+                    def _():
+                        for a in range(2):
+                            for j in range(1, rep_count):
+                                across(a, way, d, j).wait()
+
+    send_weights(0)
 
     parts = []
     for a in range(2):
@@ -234,11 +280,8 @@
                 part_send.at[a, k - 1], part_recv.at[a, k - 1], **member(k),
             )))
 
-    for k in range(2, fs_count - 1):
-        send_weights(k)
-    for k in near:
-        pass_weights(k)
-
+    for d in range(1, 2):
+        pass_weights(d)
     for copy in parts:
         copy.wait_recv()
     squares = jnp.zeros((rows, width), jnp.float32)
@@ -273,6 +316,8 @@
         ))
         for k in range(1, group)
     ]
+    for d in range(2, 3):
+        pass_weights(d)
     for copy in moment_loads:
         copy.wait()
     for copy in group_copies:
@@ -290,12 +335,14 @@
         ))
         for k in range(1, group)
     ]
-    for k in range(2, fs_count - 1):
-        pass_weights(k)
-    for copy in owned_copies + turn_copies + side:
+    for d in range(3, fs_count):
+        pass_weights(d)
+    for copy in owned_copies + turn_copies:
+
         copy.wait_recv()
     for copy in sent:
         copy.wait_send()
+    settle_weights()
 
 
 def finish(
@@ -383,8 +430,8 @@
             pltpu.VMEM((tp_count, 8, 128), f32),
             pltpu.VMEM((group, 8, 128), f32),
             dma((14,)),
-            dma((2, fs_count - 1)), dma((2, fs_count - 1)),
-            dma((2, fs_count - 1, rep_count - 1)), dma((2, fs_count - 1, rep_count - 1)),
+            dma((2, 2, fs_count - 1)), dma((2, 2, fs_count - 1)),
+            dma((2, 2, fs_count - 1, rep_count - 1)), dma((2, 2, fs_count - 1, rep_count - 1)),
             dma((2, group - 1)), dma((2, group - 1)),
             dma((tp_count - 1,)), dma((tp_count - 1,)),
             dma((group - 1,)), dma((group - 1,)),
@@ -392,7 +439,7 @@
             dma((group - 1,)), dma((group - 1,)),
         ],
         compiler_params=pltpu.CompilerParams(
-            collective_id=0, has_side_effects=True, vmem_limit_bytes=32 * 1024 * 1024
+            collective_id=0, has_side_effects=True, vmem_limit_bytes=60 * 1024 * 1024
         ),
         name="exchange",
     )(
@@ -410,7 +457,7 @@
         ),
         in_specs=[in_vmem] * 13,
         out_specs=(in_vmem,) * 10,
-        compiler_params=pltpu.CompilerParams(vmem_limit_bytes=32 * 1024 * 1024),
+        compiler_params=pltpu.CompilerParams(vmem_limit_bytes=60 * 1024 * 1024),
         name="finish",
     )(
         direction, owned, clip, all_value, all_output, basis_value, basis_output,

time: 66.5 us -> 45.4 us (0.68)
  local copies, waits for them, and re-layouts: 13.3 us -> 0 us
  Pallas kernels: 51.8 us -> 44.6 us
    unnamed x24 -> x0, local copies, waits for them, and re-layouts: 13.3 us -> none
    pallas_call x1, Pallas kernels: 48.9 us -> 39.9 us  [kernels(): pl.pallas_call(functools.partial(exchange, fs_count, rep_count, tp_count)...]
    pallas_call x1, Pallas kernels: 2.87 us -> 4.65 us  [kernels(): pl.pallas_call(finish, out_shape=(shape((count, width), f32), shape((widt...]
where the time goes in v2:
time: 45.4 us; the launch traced here: 45.2 us
  Pallas kernels  44.6 us (98%)
  between operations  0.65 us (1%)
    pallas_call x1, Pallas kernels, kernels(): pl.pallas_call(functools.partial(exchange, fs_count, rep_count, tp_count)...  39.9 us
    pallas_call x1, Pallas kernels, kernels(): pl.pallas_call(finish, out_shape=(shape((count, width), f32), shape((widt...  4.65 us

profile of v2, /device:TPU:0, one launch (start us, length us, event | category | flops | bytes accessed | tf_op | source)
XLA Modules:
  0.0 45.2 jit_solution(12304974883015395156)
XLA Ops:
  0.6 39.9 %exchange.1 = (bf16[8,2,16,256]{3,2,1,0:T(8,128)(2,1)}, f32[2,2,16,256]{3,2,1,0:T(8,128)}, f32[8,128]{1,0:T(8,128)}, bf16[4,512,256]{2,1,0:T(8,128)(2,1)}, bf16[4,256,512]{2,1,0:T(8,128)(2,1)}) custom-call(bf16[896,2048]{1,0:T(8,128)(2,1)} %hidden.1, bf16[896,256]{1,0:T(8,128)(2,1)} %grad_value.1, bf16[896,256]{1,0:T(8,128)(2,1)} %mixed.1, ...), custom_call_target="tpu_custom_call" | custom-call | tf_op jit(solution)/shard_map/exchange/pallas_call | solution.py:410
  40.6 4.7 %finish.1 = (f32[512,256]{1,0:T(8,128)}, f32[256,512]{1,0:T(8,128)}, f32[512,256]{1,0:T(8,128)}, f32[256,512]{1,0:T(8,128)}, bf16[2048,256]{1,0:T(8,128)(2,1)}, ...) custom-call(bf16[8,2,16,256]{3,2,1,0:T(8,128)(2,1)} %get-tuple-eleme, ...), custom_call_target="tpu_custom_call" | custom-call | tf_op jit(solution)/shard_map/finish/pallas_call | solution.py:450

commit v3 on v2

--- a/solution.py
+++ b/solution.py
@@ -118,9 +118,9 @@
     first_value, second_value, first_output, second_output,
     direction, owned, clip, all_value, all_output,
     tokens_in, thin_in, basis_in, value_in, output_in, moment_in,
-    part, landed, squares_tp, squares_group,
+    part, landed, squares_all,
     load_sem, near_send, near_recv, side_send, side_recv, part_send, part_recv,
-    tp_send, tp_recv, group_send, group_recv, owned_send, owned_recv, turn_send, turn_recv,
+    square_send, square_recv, owned_send, owned_recv, turn_send, turn_recv,
 ):
     group = fs_count * rep_count
     fs, rep, tp = lax.axis_index("fs"), lax.axis_index("rep"), lax.axis_index("tp")
@@ -160,17 +160,22 @@
         return {"fs": other // rep_count, "rep": lax.rem(other, rep_count)}
 
     barrier = pltpu.get_barrier_semaphore()
-    for k in range(1, group):
-        pl.semaphore_signal(barrier, inc=1, device_id=member(k), device_id_type=MESH)
-    for k in range(1, tp_count):
-        pl.semaphore_signal(
-            barrier, inc=1, device_id={"tp": lax.rem(tp + k, tp_count)}, device_id_type=MESH
-        )
+    everyone = group * tp_count
+
+    def anyone(k):
+        other = lax.rem(me * tp_count + tp + k, everyone)
+        place = other // tp_count
+        return {
+            "fs": place // rep_count, "rep": lax.rem(place, rep_count), "tp": lax.rem(other, tp_count)
+        }
+
+    for k in range(1, everyone):
+        pl.semaphore_signal(barrier, inc=1, device_id=anyone(k), device_id_type=MESH)
     for copy in weight_loads:
         copy.wait()
     all_value[fs] = value_in[...].astype(jnp.bfloat16)
     all_output[fs] = output_in[...].astype(jnp.bfloat16)
-    pl.semaphore_wait(barrier, group - 1 + tp_count - 1)
+    pl.semaphore_wait(barrier, everyone - 1)
 
     share_value = value_in.shape[0] // rep_count
     share_output = output_in.shape[0] // rep_count
@@ -291,13 +296,14 @@
             summed = summed + landed[a, k]
         owned[rep, a] = summed
         squares = squares + summed * summed
-    squares_tp[0] = jnp.full(squares_tp.shape[1:], jnp.sum(squares), jnp.float32)
-    tp_copies = [
+    place = me * tp_count + tp
+    squares_all[place] = jnp.full(squares_all.shape[1:], jnp.sum(squares), jnp.float32)
+    square_copies = [
         send(remote(
-            squares_tp.at[0], squares_tp.at[k], tp_send.at[k - 1], tp_recv.at[k - 1],
-            tp=lax.rem(tp + k, tp_count),
+            squares_all.at[place], squares_all.at[place],
+            square_send.at[k - 1], square_recv.at[k - 1], **anyone(k),
         ))
-        for k in range(1, tp_count)
+        for k in range(1, everyone)
     ]
     owned_copies = [
         send(remote(
@@ -306,25 +312,15 @@
         ))
         for j in range(1, rep_count)
     ]
-    for copy in tp_copies:
-        copy.wait_recv()
-    squares_group[me] = jnp.sum(squares_tp[...], axis=0)
-    group_copies = [
-        send(remote(
-            squares_group.at[me], squares_group.at[me], group_send.at[k - 1], group_recv.at[k - 1],
-            **member(k),
-        ))
-        for k in range(1, group)
-    ]
     for d in range(2, 3):
         pass_weights(d)
     for copy in moment_loads:
         copy.wait()
-    for copy in group_copies:
+    for copy in square_copies:
         copy.wait_recv()
-    mean_square = jnp.sum(squares_group[...], axis=0) / (2 * RANK * AW)
+    mean_square = jnp.sum(squares_all[...], axis=0) / (2 * RANK * AW)
     factor = jnp.minimum(1.0, 1.0 / jnp.sqrt(mean_square + norm_epsilon))
-    clip[...] = factor
+    clip[...] = jnp.broadcast_to(factor, clip.shape)
     scale = factor[:1, :1]
     for a in range(2):
         _, _, turned = moments(owned[rep, a], moment_in[a], moment_in[2 + a], scale)
@@ -345,51 +341,90 @@
     settle_weights()
 
 
-def finish(
-    direction, owned, clip, all_value, all_output, basis_value, basis_output,
-    weight_value, weight_output, first_value, second_value, first_output, second_output,
-    step_value, step_output, new_weight_value, new_weight_output, copy_value, copy_output,
-    new_first_value, new_second_value, new_first_output, new_second_output,
-):
+def finish(*refs):
+    sources, targets, inside, made = refs[:13], refs[13:23], refs[23:36], refs[36:46]
+    load_sem, store_sem = refs[46:]
+    (
+        direction, owned, clip, all_value, all_output, basis_value, basis_output,
+        weight_value, weight_output, first_value, second_value, first_output, second_output,
+    ) = inside
+    fs_count = all_value.shape[0]
     fs = lax.axis_index("fs")
     count = weight_value.shape[0]
     width = weight_value.shape[1]
+    loads = [
+        pltpu.make_async_copy(sources[i], inside[i], load_sem.at[i]) for i in range(len(inside))
+    ]
+    for i in (0, 5, 7, 6, 8, 3, 4, 1, 2, 9, 10, 11, 12):
+        loads[i].start()
+    stores = []
+
+    def store(i, here=None):
+        source, target = made[i], targets[i]
+        if here is not None:
+            source, target = source.at[here], target.at[here]
+        copy = pltpu.make_async_copy(source, target, store_sem.at[len(stores)])
+        copy.start()
+        stores.append(copy)
+
+    def ready(*which):
+        for i in which:
+            loads[i].wait()
+
+    across = (((1,), (1,)), ((), ()))
+    mine = pl.ds(pl.multiple_of(fs * count, count), count)
+    ready(0, 5)
+    turn_value = direction[:, 0].reshape(RANK, width)
+    turn_output = direction[:, 1].reshape(RANK, width).astype(jnp.float32).T.astype(jnp.bfloat16)
+
+    def value_step(rows_here):
+        return jnp.dot(basis_value[rows_here], turn_value, preferred_element_type=jnp.float32)
+
+    def output_step(rows_here):
+        return lax.dot_general(
+            turn_output, basis_output[rows_here], across, preferred_element_type=jnp.float32
+        )
+
+    step = value_step(mine)
+    made[0][...] = step
+    store(0)
+    ready(7)
+    made[2][...] = weight_value[...] - learning_rate * step
+    store(2)
+    ready(6)
+    step = output_step(mine)
+    made[1][...] = step
+    store(1)
+    ready(8)
+    made[3][...] = weight_output[...] - learning_rate * step
+    store(3)
+    ready(3)
+    for f in range(fs_count):
+        here = pl.ds(f * count, count)
+        made[4][here] = (
+            all_value[f].astype(jnp.float32) - learning_rate * value_step(here)
+        ).astype(jnp.bfloat16)
+        store(4, here)
+    ready(4)
+    for f in range(fs_count):
+        here = pl.ds(f * count, count)
+        made[5][:, here] = (
+            all_output[f].astype(jnp.float32) - learning_rate * output_step(here)
+        ).astype(jnp.bfloat16)
+        store(5, (slice(None), here))
+    ready(1, 2, 9, 10, 11, 12)
     scale = clip[:1, :1]
-    outputs = ((new_first_value, new_second_value), (new_first_output, new_second_output))
     for a, (first, second) in enumerate(
         ((first_value, second_value), (first_output, second_output))
     ):
         projected = owned[:, a].reshape(first.shape)
         new_first, new_second, _ = moments(projected, first[...], second[...], scale)
-        outputs[a][0][...] = new_first
-        outputs[a][1][...] = new_second
-    turn_value = direction[:, 0].reshape(RANK, width)
-    turn_output = direction[:, 1].reshape(RANK, width).astype(jnp.float32).T.astype(jnp.bfloat16)
-    across = (((1,), (1,)), ((), ()))
-
-    def value_step(rows_here):
-        return jnp.dot(basis_value[rows_here], turn_value, preferred_element_type=jnp.float32)
-
-    def output_step(rows_here):
-        return lax.dot_general(
-            turn_output, basis_output[rows_here], across, preferred_element_type=jnp.float32
-        )
-
-    mine = pl.ds(pl.multiple_of(fs * count, count), count)
-    step = value_step(mine)
-    step_value[...] = step
-    new_weight_value[...] = weight_value[...] - learning_rate * step
-    step = output_step(mine)
-    step_output[...] = step
-    new_weight_output[...] = weight_output[...] - learning_rate * step
-    for f in range(all_value.shape[0]):
-        here = pl.ds(f * count, count)
-        copy_value[here] = (
-            all_value[f].astype(jnp.float32) - learning_rate * value_step(here)
-        ).astype(jnp.bfloat16)
-        copy_output[:, here] = (
-            all_output[f].astype(jnp.float32) - learning_rate * output_step(here)
-        ).astype(jnp.bfloat16)
+        made[6 + 2 * a][...] = new_first
+        made[7 + 2 * a][...] = new_second
+        store(6 + 2 * a)
+        store(7 + 2 * a)
+    for copy in stores:
+        copy.wait()
 
 
 def kernels(
@@ -427,14 +462,12 @@
             pltpu.VMEM((4, rows, width), f32),
             pltpu.VMEM((2, group, rows, width), f32),
             pltpu.VMEM((2, group - 1, rows, width), f32),
-            pltpu.VMEM((tp_count, 8, 128), f32),
-            pltpu.VMEM((group, 8, 128), f32),
+            pltpu.VMEM((group * tp_count, 1, 128), f32),
             dma((14,)),
             dma((2, 2, fs_count - 1)), dma((2, 2, fs_count - 1)),
             dma((2, 2, fs_count - 1, rep_count - 1)), dma((2, 2, fs_count - 1, rep_count - 1)),
             dma((2, group - 1)), dma((2, group - 1)),
-            dma((tp_count - 1,)), dma((tp_count - 1,)),
-            dma((group - 1,)), dma((group - 1,)),
+            dma((group * tp_count - 1,)), dma((group * tp_count - 1,)),
             dma((rep_count - 1,)), dma((rep_count - 1,)),
             dma((group - 1,)), dma((group - 1,)),
         ],
@@ -447,22 +480,26 @@
         weight_value, weight_output, first_value, second_value, first_output, second_output,
     )
     moment = shape(first_value.shape, f32)
+    operands = (
+        direction, owned, clip, all_value, all_output, basis_value, basis_output,
+        weight_value, weight_output, first_value, second_value, first_output, second_output,
+    )
+    results = (
+        shape((count, width), f32), shape((width, count), f32),
+        shape((count, width), f32), shape((width, count), f32),
+        shape((model, width), bf16), shape((width, model), bf16),
+        moment, moment, moment, moment,
+    )
     return pl.pallas_call(
         finish,
-        out_shape=(
-            shape((count, width), f32), shape((width, count), f32),
-            shape((count, width), f32), shape((width, count), f32),
-            shape((model, width), bf16), shape((width, model), bf16),
-            moment, moment, moment, moment,
-        ),
-        in_specs=[in_vmem] * 13,
-        out_specs=(in_vmem,) * 10,
+        out_shape=results,
+        in_specs=[anywhere] * len(operands),
+        out_specs=(anywhere,) * len(results),
+        scratch_shapes=[pltpu.VMEM(x.shape, x.dtype) for x in operands + results]
+        + [dma((len(operands),)), dma((len(results) - 2 + 2 * fs_count,))],
         compiler_params=pltpu.CompilerParams(vmem_limit_bytes=60 * 1024 * 1024),
         name="finish",
-    )(
-        direction, owned, clip, all_value, all_output, basis_value, basis_output,
-        weight_value, weight_output, first_value, second_value, first_output, second_output,
-    )
+    )(*operands)
 
 
 def solution(mesh):

time: 45.4 us -> 43.2 us (0.952)
  Pallas kernels: 44.6 us -> 42.4 us
    pallas_call x1, Pallas kernels: 39.9 us -> 38.5 us  [kernels(): pl.pallas_call(functools.partial(exchange, fs_count, rep_count, tp_count)...]
    pallas_call x1, Pallas kernels: 4.65 us -> 3.88 us  [kernels(): pl.pallas_call(finish, out_shape=results, in_specs=[anywhere] * len(opera...]
where the time goes in v3:
time: 43.2 us; the launch traced here: 43 us
  Pallas kernels  42.4 us (98%)
  between operations  0.65 us (2%)
    pallas_call x1, Pallas kernels, kernels(): pl.pallas_call(functools.partial(exchange, fs_count, rep_count, tp_count)...  38.5 us
    pallas_call x1, Pallas kernels, kernels(): pl.pallas_call(finish, out_shape=results, in_specs=[anywhere] * len(opera...  3.88 us

profile of v3, /device:TPU:0, one launch (start us, length us, event | category | flops | bytes accessed | tf_op | source)
XLA Modules:
  0.0 43.0 jit_solution(16070069158896096645)
XLA Ops:
  0.6 38.5 %exchange.1 = (bf16[8,2,16,256]{3,2,1,0:T(8,128)(2,1)}, f32[2,2,16,256]{3,2,1,0:T(8,128)}, f32[8,128]{1,0:T(8,128)}, bf16[4,512,256]{2,1,0:T(8,128)(2,1)}, bf16[4,256,512]{2,1,0:T(8,128)(2,1)}) custom-call(bf16[896,2048]{1,0:T(8,128)(2,1)} %hidden.1, bf16[896,256]{1,0:T(8,128)(2,1)} %grad_value.1, bf16[896,256]{1,0:T(8,128)(2,1)} %mixed.1, ...), custom_call_target="tpu_custom_call" | custom-call | tf_op jit(solution)/shard_map/exchange/pallas_call | solution.py:445
  39.2 3.9 %finish.1 = (f32[512,256]{1,0:T(8,128)}, f32[256,512]{1,0:T(8,128)}, f32[512,256]{1,0:T(8,128)}, f32[256,512]{1,0:T(8,128)}, bf16[2048,256]{1,0:T(8,128)(2,1)}, ...) custom-call(bf16[8,2,16,256]{3,2,1,0:T(8,128)(2,1)} %get-tuple-eleme, ...), custom_call_target="tpu_custom_call" | custom-call | tf_op jit(solution)/shard_map/finish/pallas_call | solution.py:493
